TPU v7x, 32 devices: a whole 2x2x4 slice. The times are simulated.
32 devices in a mesh: fs: 8 (over z, y), tp: 4 (over x, core).
Axes of the slice: x: 2, y: 2, z: 4, core: 2. Of those that a mesh axis runs over, the one named last changes fastest.
Arguments:
- cotangent: bfloat16 [5120, 1024], P('fs', 'tp'), may hold values from -6 to 6
- inputs: bfloat16 [5120, 1024], P('fs', 'tp'), may hold values from -6 to 6
- pre_act: bfloat16 [5120, 2112], P('fs'), may hold values from -6 to 6
- w_up: bfloat16 [2112, 1024], P('fs', 'tp'), may hold values from -0.1875 to 0.1875
- w_down: bfloat16 [2112, 1024], P('fs', 'tp'), may hold values from -0.125 to 0.125
Outputs:
- grad_input: bfloat16 [5120, 1024], P('fs', 'tp')
- grad_up: float32 [2112, 1024], P('fs', 'tp')
All inputs are finite; a program needn't handle non-finite values.
Results may differ from a plain program's by a relative error of at most 0.0049.
Values may be sent and summed in bfloat16 or wider, within the bound.
A program may use at most 64 MiB of HBM per device.

v0:
```python
import jax
import jax.numpy as jnp
from jax import lax
from jax.sharding import PartitionSpec as P


def times_rows(left, piece):
    return lax.dot_general(
        left, piece, (((1,), (1,)), ((), ())), preferred_element_type=jnp.float32
    )


def local(cotangent, inputs, pre_act, w_up, w_down):
    row_count = cotangent.shape[0]
    token_total = row_count * lax.axis_size("fs")
    full_cotangent = lax.all_gather(cotangent, "tp", axis=1, tiled=True)
    down_whole = lax.all_gather(w_down, "tp", axis=1, tiled=True)
    grad_hidden = times_rows(full_cotangent, lax.all_gather(down_whole, "fs", axis=0, tiled=True))
    grad_pre = (2.0 * grad_hidden * jnp.maximum(pre_act.astype(jnp.float32), 0.0)).astype(
        jnp.bfloat16
    )
    columns = grad_pre
    grad_input = jnp.dot(
        columns, lax.all_gather(w_up, "fs", axis=0, tiled=True), preferred_element_type=jnp.float32
    )
    columns = grad_pre
    grad_share = lax.psum_scatter(
        lax.dot_general(
            columns, inputs, (((0,), (0,)), ((), ())), preferred_element_type=jnp.float32
        ),
        "fs",
        scatter_dimension=0,
        tiled=True,
    )
    grad_up = grad_share / jnp.sqrt(jnp.float32(token_total))
    return (grad_input.astype(jnp.bfloat16), grad_up)


def solution(mesh):
    return jax.shard_map(
        local,
        mesh=mesh,
        in_specs=(P("fs", "tp"), P("fs", "tp"), P("fs", None), P("fs", "tp"), P("fs", "tp")),
        out_specs=(P("fs", "tp"), P("fs", "tp")),
        check_vma=False,
    )
```

profile of v0, /device:TPU:0, one launch (start us, length us, event | category | flops | bytes accessed | tf_op | source)
XLA Modules:
  0.0 227.8 jit_solution(900045571831877215)
XLA Ops:
  7.2 0.0 copy-start
  7.2 0.0 all-gather.4.cloned.1.call-start
  7.2 0.7 all-gather.4.cloned.1.call-update
  7.9 0.0 all-gather.6.cloned.1.call-start
  8.0 10.3 %all_gather.13 = bf16[264,1024]{1,0:T(8,128)(2,1)} all-gather(bf16[264,256]{1,0:T(8,128)(2,1)} %param.9), channel_id=1, replica_groups=mesh['fs'=8,'tp'=4] {'tp'}, dimensions={1}, use_global_device_ids=true | all-gather | bytes 675840 | tf_op jit(solution)/shard_map/all_gather | solution.py:17
  18.3 0.0 all-gather.6.cloned.1.call-update
  18.3 0.0 all-gather.8.cloned.1.call-start
  18.4 0.7 all-gather.8.cloned.1.call-update
  19.1 0.0 reduce-scatter.2.cloned.1.call-start
  19.1 11.5 %all-gather.4.cloned.1.call-done = bf16[640,1024]{1,0:T(8,128)(2,1)} async-done(((bf16[640,256]{1,0:T(8,128)(2,1)}), bf16[640,1024]{1,0:T(8,128)(2,1)}) %all-gather.4.cloned.1.call-update) | async-done | bytes 1310736 | tf_op jit(solution)/shard_map/all_gather | solution.py:16
  30.6 76.6 %all-gather.6.cloned.1.call-done = bf16[2112,1024]{1,0:T(8,128)(2,1)} async-done(((bf16[264,1024]{1,0:T(8,128)(2,1)}), bf16[2112,1024]{1,0:T(8,128)(2,1)}) %all-gather.6.cloned.1.call-update) | async-done | bytes 4325392 | tf_op jit(solution)/shard_map/all_gather | solution.py:18
  107.2 7.1 %fusion.1 = bf16[640,2112]{0,1:T(8,128)(2,1)S(1)} fusion(bf16[640,2112]{0,1:T(8,128)(2,1)} %param.7, bf16[640,1024]{1,0:T(8,128)(2,1)} %all-gather.4.cloned.1.call-done, bf16[2112,1024]{1,0:T(8,128)(2,1)} %all-gather.6.cloned.1.call-done), kind=kOutput, calls=%fused_computation.2 | convolution fusion | flops 2774999040 | bytes 11042816 | tf_op jit(solution)/shard_map/dot_general | solution.py:8
  114.4 0.0 copy-done
  114.4 2.4 %fusion.2 = f32[2112,256]{1,0:T(8,128)} fusion(bf16[640,2112]{0,1:T(8,128)(2,1)S(1)} %fusion.1, bf16[640,256]{1,0:T(8,128)(2,1)S(1)} %copy-done), kind=kOutput, calls=%fused_computation.5 | convolution fusion | flops 692060160 | bytes 5193728 | tf_op jit(solution)/shard_map/dot_general | solution.py:28
  116.7 0.0 reduce-scatter.2.cloned.1.call-update
  116.8 31.7 %all-gather.8.cloned.1.call-done = bf16[2112,256]{1,0:T(8,128)(2,1)} async-done(((bf16[264,256]{1,0:T(8,128)(2,1)}), bf16[2112,256]{1,0:T(8,128)(2,1)}) %all-gather.8.cloned.1.call-update) | async-done | bytes 1081360 | tf_op jit(solution)/shard_map/all_gather | solution.py:24
  148.5 2.9 %convolution_convert_fusion = bf16[640,256]{1,0:T(8,128)(2,1)} fusion(bf16[640,2112]{0,1:T(8,128)(2,1)S(1)} %fusion.1, bf16[2112,256]{1,0:T(8,128)(2,1)} %all-gather.8.cloned.1.call-done), kind=kOutput, calls=%fused_computation.3 | convolution fusion | flops 692224000 | bytes 4112384 | tf_op jit(solution)/shard_map/dot_general | solution.py:23
  151.4 68.2 %reduce-scatter.2.cloned.1.call-done = f32[264,256]{1,0:T(8,128)} async-done(((f32[2112,256]{1,0:T(8,128)}), f32[264,256]{1,0:T(8,128)}) %reduce-scatter.2.cloned.1.call-update) | async-done | bytes 270352 | tf_op jit(solution)/shard_map/reduce_scatter | solution.py:27
  219.6 1.7 broadcast_multiply_fusion
Async XLA Ops:
  7.2 107.2 %copy-start = (bf16[640,256]{1,0:T(8,128)(2,1)S(1)}, bf16[640,256]{1,0:T(8,128)(2,1)}, u32[]{:S(2)}) copy-start(bf16[640,256]{1,0:T(8,128)(2,1)} %param.6) | copy-start | bytes 983044
  7.2 23.4 %all-gather.4.cloned.1.call-start = ((), (), s32[]{:S(2)}) async-start(), calls=%async_computation.1 | async-start | bytes 1638400 | tf_op jit(solution)/shard_map/all_gather | solution.py:16
  7.9 99.3 %all-gather.6.cloned.1.call-start = ((), (), s32[]{:S(2)}) async-start(), calls=%async_computation.2 | async-start | bytes 4866048 | tf_op jit(solution)/shard_map/all_gather | solution.py:18
  18.3 130.1 %all-gather.8.cloned.1.call-start = ((), (), s32[]{:S(2)}) async-start(), calls=%async_computation.3 | async-start | bytes 1216512 | tf_op jit(solution)/shard_map/all_gather | solution.py:24
  19.1 200.5 %reduce-scatter.2.cloned.1.call-start = ((), (), s32[]{:S(2)}) async-start(), calls=%async_computation.4 | async-start | bytes 2433024 | tf_op jit(solution)/shard_map/reduce_scatter | solution.py:27
Sparse Core Ops, SparseCore 0:
  9.5 21.0 all-gather.3
  32.8 74.3 all-gather.5
  109.4 39.0 all-gather.7
  151.8 67.7 reduce-scatter.1
where the time goes:
time: 228 us
  waiting for transfers between devices  189 us (83%)
  between operations  13.8 us (6%)
  matrix products  12.4 us (5%)
  blocking collectives  10.3 us (5%)
    all_gather x1, waiting for transfers between devices, local(): lax.all_gather(down_whole, 'fs', axis=0, tiled=True)  76.6 us
    reduce_scatter x1, waiting for transfers between devices, local(): lax.psum_scatter(lax.dot_general(columns, inputs, (((0,), (0,)), ((), ())...  68.2 us
    all_gather x1, waiting for transfers between devices, local(): lax.all_gather(w_up, 'fs', axis=0, tiled=True)  31.7 us
    all_gather x1, waiting for transfers between devices, local(): full_cotangent = lax.all_gather(cotangent, 'tp', axis=1, tiled=True)  11.5 us
    all_gather x1, blocking collectives, local(): down_whole = lax.all_gather(w_down, 'tp', axis=1, tiled=True)  10.3 us
    dot_general x1, matrix products, times_rows(): lax.dot_general(left, piece, (((1,), (1,)), ((), ())), preferred_element_...  7.12 us
  transfers between devices with their start and end apart: 4, of which 4 were waited for; matrix products, arithmetic and copies ran while one was open for 5% of the time, Pallas kernels for 0%

commit v1 on v0

--- a/solution.py
+++ b/solution.py
@@ -2,6 +2,16 @@
 import jax.numpy as jnp
 from jax import lax
 from jax.sharding import PartitionSpec as P
+
+
+def gather_by_hops(shard, mesh_axis, d):
+    n_dev = lax.axis_size(mesh_axis)
+    held, tiles = (shard, [shard])
+    for _ in range(n_dev - 1):
+        held = lax.ppermute(held, mesh_axis, [(i, (i + 1) % n_dev) for i in range(n_dev)])
+        tiles.insert(0, held)
+    line = jnp.concatenate(tiles, axis=d)
+    return jnp.roll(line, (lax.axis_index(mesh_axis) + 1) * shard.shape[d], axis=d)
 
 
 def times_rows(left, piece):
@@ -13,7 +23,7 @@
 def local(cotangent, inputs, pre_act, w_up, w_down):
     row_count = cotangent.shape[0]
     token_total = row_count * lax.axis_size("fs")
-    full_cotangent = lax.all_gather(cotangent, "tp", axis=1, tiled=True)
+    full_cotangent = gather_by_hops(cotangent, "tp", 1)
     down_whole = lax.all_gather(w_down, "tp", axis=1, tiled=True)
     grad_hidden = times_rows(full_cotangent, lax.all_gather(down_whole, "fs", axis=0, tiled=True))
     grad_pre = (2.0 * grad_hidden * jnp.maximum(pre_act.astype(jnp.float32), 0.0)).astype(

time: 228 us -> 213 us (0.934)
  waiting for transfers between devices: 189 us -> 168 us
  local copies, waits for them, and re-layouts: 0.01 us -> 6.31 us
    all_gather x1, waiting for transfers between devices: 76.6 us -> 48.8 us  [local(): lax.all_gather(down_whole, 'fs', axis=0, tiled=True)]
    ppermute x0 -> x3, waiting for transfers between devices: none -> 19.3 us  [gather_by_hops(): lax.ppermute(held, mesh_axis, [(i, (i + 1) % n_dev) for i in range(n_dev)])]
    all_gather x1 -> x0, waiting for transfers between devices: 11.5 us -> none  [local(): full_cotangent = lax.all_gather(cotangent, 'tp', axis=1, tiled=True)]
    unnamed x2 -> x11, local copies, waits for them, and re-layouts: 0.01 us -> 5.52 us
  transfers between devices with their start and end apart: 4 -> 6, of which waited for: 4 -> 6; matrix products, arithmetic and copies ran while one was open for 5% -> 9% of each run, Pallas kernels for 0% -> 0%
where the time goes in v1:
time: 213 us
  waiting for transfers between devices  168 us (79%)
  between operations  13.8 us (6%)
  matrix products  12.4 us (6%)
  blocking collectives  10.5 us (5%)
  local copies, waits for them, and re-layouts  6.31 us (3%)
    reduce_scatter x1, waiting for transfers between devices, local(): lax.psum_scatter(lax.dot_general(columns, inputs, (((0,), (0,)), ((), ())...  68.3 us
    all_gather x1, waiting for transfers between devices, local(): lax.all_gather(down_whole, 'fs', axis=0, tiled=True)  48.8 us
    all_gather x1, waiting for transfers between devices, local(): lax.all_gather(w_up, 'fs', axis=0, tiled=True)  31.7 us
    ppermute x3, waiting for transfers between devices, gather_by_hops(): lax.ppermute(held, mesh_axis, [(i, (i + 1) % n_dev) for i in range(n_dev)])  19.3 us
    all_gather x1, blocking collectives, local(): down_whole = lax.all_gather(w_down, 'tp', axis=1, tiled=True)  10.5 us
    dot_general x1, matrix products, times_rows(): lax.dot_general(left, piece, (((1,), (1,)), ((), ())), preferred_element_...  7.12 us
    unnamed x11, local copies, waits for them, and re-layouts  5.52 us
  transfers between devices with their start and end apart: 6, of which 6 were waited for; matrix products, arithmetic and copies ran while one was open for 9% of the time, Pallas kernels for 0%

profile of v1, /device:TPU:0, one launch (start us, length us, event | category | flops | bytes accessed | tf_op | source)
XLA Modules:
  0.0 213.3 jit_solution(4555875753944493104)
XLA Ops:
  7.2 0.0 copy-start
  7.2 0.0 copy-start.1
  7.2 0.0 all-gather.3.cloned.1.call-start
  7.2 10.5 %all_gather.9 = bf16[264,1024]{1,0:T(8,128)(2,1)} all-gather(bf16[264,256]{1,0:T(8,128)(2,1)} %param.9), channel_id=1, replica_groups=mesh['fs'=8,'tp'=4] {'tp'}, dimensions={1}, use_global_device_ids=true | all-gather | bytes 675840 | tf_op jit(solution)/shard_map/all_gather | solution.py:27
  17.7 0.0 all-gather.3.cloned.1.call-update
  17.7 0.0 all-gather.5.cloned.1.call-start
  17.8 0.4 collective-permute-start
  18.2 6.4 %collective-permute-done = bf16[640,256]{1,0:T(8,128)(2,1)S(1)} collective-permute-done((bf16[640,256]{1,0:T(8,128)(2,1)}, bf16[640,256]{1,0:T(8,128)(2,1)S(1)}, u32[]{:S(2)}, u32[]{:S(2)}) %collective-permute-start) | collective-permute-done | bytes 327712 | tf_op jit(solution)/shard_map/ppermute | solution.py:11
  24.5 0.0 collective-permute-start.1
  24.5 6.5 %collective-permute-done.1 = bf16[640,256]{1,0:T(8,128)(2,1)S(1)} collective-permute-done((bf16[640,256]{1,0:T(8,128)(2,1)S(1)}, bf16[640,256]{1,0:T(8,128)(2,1)S(1)}, u32[]{:S(2)}, u32[]{:S(2)}) %collective-permute-start.1) | collective-permute-done | bytes 327712 | tf_op jit(solution)/shard_map/ppermute | solution.py:11
  31.0 0.0 collective-permute-start.2
  31.0 0.0 all-gather.5.cloned.1.call-update
  31.1 0.0 reduce-scatter.2.cloned.1.call-start
  31.1 6.4 %collective-permute-done.2 = bf16[640,256]{1,0:T(8,128)(2,1)S(1)} collective-permute-done((bf16[640,256]{1,0:T(8,128)(2,1)S(1)}, bf16[640,256]{1,0:T(8,128)(2,1)S(1)}, u32[]{:S(2)}, u32[]{:S(2)}) %collective-permute-start.2) | collective-permute-done | bytes 327712 | tf_op jit(solution)/shard_map/ppermute | solution.py:11
  37.5 0.8 constant_dynamic-update-slice_fusion.7
  38.3 0.8 constant_dynamic-update-slice_fusion.6
  39.1 0.8 constant_dynamic-update-slice_fusion.5
  39.9 0.0 copy-done.1
  39.9 0.8 constant_dynamic-update-slice_fusion.4
  40.7 0.8 constant_dynamic-update-slice_fusion.3
  41.5 0.8 constant_dynamic-update-slice_fusion.2
  42.3 0.8 constant_dynamic-update-slice_fusion.1
  43.1 0.8 constant_dynamic-update-slice_fusion
  43.8 48.8 %all-gather.3.cloned.1.call-done = bf16[2112,1024]{1,0:T(8,128)(2,1)} async-done(((bf16[264,1024]{1,0:T(8,128)(2,1)}), bf16[2112,1024]{1,0:T(8,128)(2,1)}) %all-gather.3.cloned.1.call-update) | async-done | bytes 4325392 | tf_op jit(solution)/shard_map/all_gather | solution.py:28
  92.6 7.1 %fusion.1 = bf16[640,2112]{0,1:T(8,128)(2,1)S(1)} fusion(bf16[640,2112]{0,1:T(8,128)(2,1)} %param.7, bf16[2112,1024]{1,0:T(8,128)(2,1)} %all-gather.3.cloned.1.call-done, bf16[640,2048]{1,0:T(8,128)(2,1)} %constant_dynamic-update-slice_fusion, s32[]{:T(128)S(6)} %select_n.14), kind=kOutput, calls=%fused_computation.2 | convolution fusion | flops 2774999040 | bytes 11042820 | tf_op jit(solution)/shard_map/dot_general | solution.py:18
  99.7 0.0 copy-done
  99.8 2.4 %fusion.4 = f32[2112,256]{1,0:T(8,128)} fusion(bf16[640,2112]{0,1:T(8,128)(2,1)S(1)} %fusion.1, bf16[640,256]{1,0:T(8,128)(2,1)S(1)} %copy-done), kind=kOutput, calls=%fused_computation.15 | convolution fusion | flops 692060160 | bytes 5193728 | tf_op jit(solution)/shard_map/dot_general | solution.py:38
  102.1 0.0 reduce-scatter.2.cloned.1.call-update
  102.1 31.7 %all-gather.5.cloned.1.call-done = bf16[2112,256]{1,0:T(8,128)(2,1)} async-done(((bf16[264,256]{1,0:T(8,128)(2,1)}), bf16[2112,256]{1,0:T(8,128)(2,1)}) %all-gather.5.cloned.1.call-update) | async-done | bytes 1081360 | tf_op jit(solution)/shard_map/all_gather | solution.py:34
  133.8 2.9 %convolution_convert_fusion = bf16[640,256]{1,0:T(8,128)(2,1)} fusion(bf16[640,2112]{0,1:T(8,128)(2,1)S(1)} %fusion.1, bf16[2112,256]{1,0:T(8,128)(2,1)} %all-gather.5.cloned.1.call-done), kind=kOutput, calls=%fused_computation.4 | convolution fusion | flops 692224000 | bytes 4112384 | tf_op jit(solution)/shard_map/dot_general | solution.py:33
  136.8 68.3 %reduce-scatter.2.cloned.1.call-done = f32[264,256]{1,0:T(8,128)} async-done(((f32[2112,256]{1,0:T(8,128)}), f32[264,256]{1,0:T(8,128)}) %reduce-scatter.2.cloned.1.call-update) | async-done | bytes 270352 | tf_op jit(solution)/shard_map/reduce_scatter | solution.py:37
  205.0 1.7 broadcast_multiply_fusion
Async XLA Ops:
  7.2 92.6 %copy-start = (bf16[640,256]{1,0:T(8,128)(2,1)S(1)}, bf16[640,256]{1,0:T(8,128)(2,1)}, u32[]{:S(2)}) copy-start(bf16[640,256]{1,0:T(8,128)(2,1)} %param.6) | copy-start | bytes 983044
  7.2 32.7 %copy-start.1 = (bf16[640,256]{1,0:T(8,128)(2,1)S(1)}, bf16[640,256]{1,0:T(8,128)(2,1)}, u32[]{:S(2)}) copy-start(bf16[640,256]{1,0:T(8,128)(2,1)} %param.5) | copy-start | bytes 983044
  7.2 85.4 %all-gather.3.cloned.1.call-start = ((), (), s32[]{:S(2)}) async-start(), calls=%async_computation.1 | async-start | bytes 4866048 | tf_op jit(solution)/shard_map/all_gather | solution.py:28
  17.7 116.1 %all-gather.5.cloned.1.call-start = ((), (), s32[]{:S(2)}) async-start(), calls=%async_computation.2 | async-start | bytes 1216512 | tf_op jit(solution)/shard_map/all_gather | solution.py:34
  17.8 6.8 %collective-permute-start = (bf16[640,256]{1,0:T(8,128)(2,1)}, bf16[640,256]{1,0:T(8,128)(2,1)S(1)}, u32[]{:S(2)}, u32[]{:S(2)}) collective-permute-start(bf16[640,256]{1,0:T(8,128)(2,1)} %param.5), channel_id=1, source_target_pairs={{0,1},{1,2},{2,3},{3,0},{4,5},{5,6},{6,7},{7,4},{8,9},{9,10},{10,1... | collective-permute-start | bytes 983048 | tf_op jit(solution)/shard_map/ppermute | solution.py:11
  24.5 6.5 %collective-permute-start.1 = (bf16[640,256]{1,0:T(8,128)(2,1)S(1)}, bf16[640,256]{1,0:T(8,128)(2,1)S(1)}, u32[]{:S(2)}, u32[]{:S(2)}) collective-permute-start(bf16[640,256]{1,0:T(8,128)(2,1)S(1)} %collective-permute-done), channel_id=1, source_target_pairs={{0,1},{1,2},{2,3},{3,0},{4,5},{5,6},{6,7},{7,4},{8,9},{9,10},{10,1... | collective-permute-start | bytes 983048 | tf_op jit(solution)/shard_map/ppermute | solution.py:11
  31.0 6.5 %collective-permute-start.2 = (bf16[640,256]{1,0:T(8,128)(2,1)S(1)}, bf16[640,256]{1,0:T(8,128)(2,1)S(1)}, u32[]{:S(2)}, u32[]{:S(2)}) collective-permute-start(bf16[640,256]{1,0:T(8,128)(2,1)S(1)} %collective-permute-done.1), channel_id=1, source_target_pairs={{0,1},{1,2},{2,3},{3,0},{4,5},{5,6},{6,7},{7,4},{8,9},{9,10},{10,1... | collective-permute-start | bytes 983048 | tf_op jit(solution)/shard_map/ppermute | solution.py:11
  31.1 174.0 %reduce-scatter.2.cloned.1.call-start = ((), (), s32[]{:S(2)}) async-start(), calls=%async_computation.3 | async-start | bytes 2433024 | tf_op jit(solution)/shard_map/reduce_scatter | solution.py:37
Sparse Core Ops, SparseCore 0:
  17.8 74.7 all-gather.2
  94.8 39.0 all-gather.4
  137.3 67.6 reduce-scatter.1
